TPU v7x, 32 devices: a whole 2x2x4 slice. The times are simulated.
32 devices in a mesh: ep: 8 (over z, y), tp: 4 (over x, core).
Axes of the slice: x: 2, y: 2, z: 4, core: 2. Of those that a mesh axis runs over, the one named last changes fastest.
Arguments:
- x_mix: bfloat16 [8192, 2048], P('ep'), may hold values from -6 to 6
- mix_gain: float32 [2048], replicated, may hold values from 0.1 to 1.9
- w_query: bfloat16 [2048, 1024], P(None, 'tp'), may hold values from -0.125 to 0.125
- w_key: bfloat16 [2048, 1024], P(None, 'tp'), may hold values from -0.125 to 0.125
- w_value: bfloat16 [2048, 1024], P(None, 'tp'), may hold values from -0.125 to 0.125
- w_outgate: bfloat16 [2048, 1024], P(None, 'tp'), may hold values from -0.125 to 0.125
- w_gates: bfloat16 [2048, 32], replicated, may hold values from -0.125 to 0.125
- gate_bias: float32 [4, 8], P(None, 'tp'), may hold values from -1 to 120, as said below
- gate_drift: float32 [32], P('ep'), may hold values from -1.5 to 1.5
- head_gain: float32 [1024], P('tp'), may hold values from 0.1 to 1.9
- w_out: bfloat16 [1024, 2048], P('tp'), may hold values from -0.1875 to 0.1875
- x_route: bfloat16 [4096, 2048], P('ep'), may hold values from -6 to 6
- route_gain: float32 [2048], replicated, may hold values from 0.1 to 1.9
- routes: int32 [4096, 2], P('ep'), may hold values from 0 to 7, all different within a row; in each aligned block of 128 rows (0 to 127, 128 to 255, ...) at most 64 rows name the same one
- route_weight: float32 [4096, 2], P(('ep', 'tp')), may hold values from 0.2 to 1
- w_gate_e: bfloat16 [8, 2048, 1024], P('ep', None, 'tp'), may hold values from -0.125 to 0.125
- w_up_e: bfloat16 [8, 2048, 1024], P('ep', None, 'tp'), may hold values from -0.125 to 0.125
- w_down_e: bfloat16 [8, 1024, 2048], P('ep', 'tp'), may hold values from -0.1875 to 0.1875
Outputs:
- mixer_out: bfloat16 [8192, 2048], P(('ep', 'tp'))
- route_out: bfloat16 [4096, 2048], P(('ep', 'tp'))
Inputs may be any that keep to these rules, and one draw needn't show every extreme that they name: `routes`: in each aligned block of 128 rows, no expert is named by more than 64 entries; the 2 experts of a row differ. `gate_bias`: rows 0 and 2 are input gate offsets, rows 1 and 3 forget gate offsets.
All inputs are finite; a program needn't handle non-finite values.
Results may differ from a plain program's by a relative error of at most 0.017.
Values may be sent and summed in bfloat16 or wider, within the bound.
A program may use at most 128 MiB of HBM per device.

v0:
```python
import functools

import jax
import jax.numpy as jnp
from jax import lax
from jax.experimental import pallas as pl
from jax.experimental.pallas import tpu as pltpu
from jax.sharding import PartitionSpec as P

HD = 128
TOPK = 2
BLK = 256
EPS = 1e-06
NEG = -1e30
MESH = pl.DeviceIdType.MESH
F32 = jnp.float32
BF16 = jnp.bfloat16
LANES = 128
CHUNK = 512


def nn(a, b):
    return lax.dot_general(a, b, (((1,), (0,)), ((), ())), preferred_element_type=F32)


def nt(a, b):
    return lax.dot_general(a, b, (((1,), (1,)), ((), ())), preferred_element_type=F32)


def tn(a, b):
    return lax.dot_general(a, b, (((0,), (0,)), ((), ())), preferred_element_type=F32)


def rms(rows, gain):
    rows = rows.astype(F32)
    return rows * lax.rsqrt(jnp.mean(rows * rows, axis=-1, keepdims=True) + EPS) * gain


def body(
    E, TP, heads, cap, quarter,
    x_mix, wq, wk, wv, wo, x_route, wg_e, wu_e, wd_e, w_out,
    mix_gain, route_gain, head_gain, w_gates, gate_add, routes, weights,
    mixer_out, route_out,
    xm, wqv, wkv, wvv, wov, xr, wgv, wuv, wdv, wfull, wts,
    sendbuf, xin, yboth, yrecv, retsend, ret, outsend, outrecv,
    qs, ks, vs, os_, rowsv, colsv, abuf, kvb, nb, stsend, scsend, strecv, screcv,
    cin, nin, min_, hsend, hrecv, slot_v,
    lsem, own_sem, d_send, d_recv, f_send, f_recv, y_send, y_recv, r_send, r_recv,
    s_send, s_recv, c_send, c_recv, h_send, h_recv, w_send, w_recv, g_send, g_recv, o_send, o_recv,
):
    e = lax.axis_index("ep")
    t = lax.axis_index("tp")
    lo = lax.rem(t, 2)
    hi = lax.div(t, 2)
    mate = t + 1 - 2 * lo
    H = TP // 2
    R = H * cap
    D = xm.shape[1]
    NB = xm.shape[0] // BLK
    slots = E * cap

    loads = []
    for h in range(H):
        loads.append(pltpu.make_async_copy(
            x_route.at[pl.ds((2 * h + lo) * quarter, quarter)], xr.at[h], lsem.at[h]))
    for i, (src, dst) in enumerate([
        (x_mix, xm), (wq, wqv), (wk, wkv), (wv, wvv), (wo, wov),
        (wg_e, wgv), (wu_e, wuv), (wd_e, wdv), (w_out, wfull.at[t]),
    ]):
        loads.append(pltpu.make_async_copy(src, dst, lsem.at[H + i]))
    loads.append(pltpu.make_async_copy(weights, wts.at[hi], lsem.at[H + 9]))
    for c in loads:
        c.start()

    barrier = pltpu.get_barrier_semaphore()
    for k in range(1, E):
        pl.semaphore_signal(barrier, inc=1, device_id=(lax.rem(e + k, E), t), device_id_type=MESH)
    for k in range(1, TP):
        pl.semaphore_signal(barrier, inc=1, device_id=(e, lax.rem(t + k, TP)), device_id_type=MESH)
    pl.semaphore_wait(barrier, E - 1 + TP - 1)

    tri = (lax.broadcasted_iota(jnp.int32, (quarter, quarter), 0)
           > lax.broadcasted_iota(jnp.int32, (quarter, quarter), 1)).astype(BF16)
    for h in range(H):
        loads[h].wait()
        rows = rms(xr[h], route_gain[...]).astype(BF16)
        table = routes[pl.ds((2 * h + lo) * quarter, quarter), :]
        experts = lax.broadcasted_iota(jnp.int32, (quarter, E), 1)
        hot = [(experts == table[:, j:j + 1]).astype(F32) for j in range(TOPK)]
        before = nn(tri, sum(hot).astype(BF16))
        place = lax.broadcasted_iota(jnp.int32, (quarter, slots), 1)
        pick = None
        for j in range(TOPK):
            slot = table[:, j:j + 1] * cap + jnp.sum(before * hot[j], axis=1, keepdims=True).astype(jnp.int32)
            slot_v[h, j] = jnp.broadcast_to(slot, (quarter, LANES))
            here = (place == slot).astype(F32)
            pick = here if pick is None else pick + here
        pick = pick.astype(BF16)
        for c in range(0, D, CHUNK):
            packed = tn(pick, rows[:, c:c + CHUNK]).astype(BF16)
            sendbuf[:, h * cap:(h + 1) * cap, c:c + CHUNK] = packed.reshape(E, cap, CHUNK)

    def dispatch(k):
        to = lax.rem(e + k, E)
        return pltpu.make_async_remote_copy(
            src_ref=sendbuf.at[to], dst_ref=xin.at[lo, e], send_sem=d_send.at[k], recv_sem=d_recv.at[k],
            device_id=(to, t), device_id_type=MESH)

    own = pltpu.make_async_copy(sendbuf.at[e], xin.at[lo, e], own_sem.at[0])
    own.start()
    for k in range(1, E):
        dispatch(k).start()

    loads[H + 8].wait()
    loads[H + 9].wait()

    def share_w(k):
        return pltpu.make_async_remote_copy(
            src_ref=wfull.at[t], dst_ref=wfull.at[t], send_sem=w_send.at[k], recv_sem=w_recv.at[k],
            device_id=(e, lax.rem(t + k, TP)), device_id_type=MESH)

    def share_g(k):
        return pltpu.make_async_remote_copy(
            src_ref=wts.at[hi], dst_ref=wts.at[hi], send_sem=g_send.at[k], recv_sem=g_recv.at[k],
            device_id=(e, lax.rem(t + 2 * k, TP)), device_id_type=MESH)

    for k in range(1, H):
        share_g(k).start()
    for k in range(1, TP):
        share_w(k).start()

    for i in range(5):
        loads[H + i].wait()
    pos_r = lax.broadcasted_iota(jnp.int32, (BLK, BLK), 0)
    pos_c = lax.broadcasted_iota(jnp.int32, (BLK, BLK), 1)

    def project(j, carry):
        at = pl.ds(pl.multiple_of(j * BLK, BLK), BLK)
        normed = rms(xm[at, :], mix_gain[...]).astype(BF16)
        qs[at, :] = nn(normed, wqv[...]).astype(BF16)
        k_all = (nn(normed, wkv[...]) * (HD ** -0.5)).astype(BF16)
        v_all = nn(normed, wvv[...]).astype(BF16)
        ks[at, :] = k_all
        vs[at, :] = v_all
        os_[at, :] = nn(normed, wov[...]).astype(BF16)
        pre = nt(w_gates[...], normed) + gate_add[j]
        logf = jnp.minimum(pre, 0.0) - jnp.log1p(jnp.exp(-jnp.abs(pre)))
        upper = (pos_r <= pos_c).astype(F32)
        lower = (pos_r >= pos_c).astype(F32)
        cum = jnp.dot(logf, upper, precision=lax.Precision.HIGHEST, preferred_element_type=F32)
        rev = jnp.dot(logf, lower, precision=lax.Precision.HIGHEST, preferred_element_type=F32)
        b_fw = cum[heads:2 * heads]
        b_bw = rev[3 * heads:4 * heads]
        a_fw = pre[0:heads] - b_fw
        a_bw = pre[2 * heads:3 * heads] - b_bw
        rows = jnp.concatenate([a_fw, a_bw, b_fw, b_bw], axis=0)
        cols = jnp.transpose(rows)
        rowsv[j] = rows
        colsv[j] = cols
        scal = []
        for d in range(2):
            for h in range(heads):
                i = d * heads + h
                top = jnp.max(rows[i:i + 1], axis=1, keepdims=True)
                scal.append(jnp.broadcast_to(top, (1, LANES)))
                w_col = jnp.exp(cols[:, i:i + 1] - top)
                hs = slice(h * HD, (h + 1) * HD)
                kw = k_all[:, hs].astype(F32) * w_col
                kvb[j, i] = tn(kw.astype(BF16), v_all[:, hs])
                nb[j, i:i + 1] = jnp.sum(kw, axis=0, keepdims=True)
        for d in range(2):
            for h in range(heads):
                i = 2 * heads + d * heads + h
                end = rows[i:i + 1, BLK - 1:BLK] if d == 0 else rows[i:i + 1, 0:1]
                scal.append(jnp.broadcast_to(end, (1, LANES)))
        abuf[j] = jnp.concatenate(scal, axis=0)
        return carry

    lax.fori_loop(0, NB, project, 0)

    def advance(state, i, j):
        mem, nor, m = state
        top = abuf[j, i:i + 1]
        tot = abuf[j, 2 * heads + i:2 * heads + i + 1]
        g = jnp.maximum(m, top)
        old, new = jnp.exp(m - g), jnp.exp(top - g)
        return (old * mem + new * kvb[j, i], old * nor + new * nb[j, i:i + 1], tot + g)

    def order(d):
        return range(NB) if d == 0 else range(NB - 1, -1, -1)

    for d in range(2):
        for h in range(heads):
            i = d * heads + h
            state = (jnp.zeros((HD, HD), F32), jnp.zeros((1, HD), F32), jnp.full((1, LANES), NEG, F32))
            total = jnp.zeros((1, LANES), F32)
            for j in order(d):
                state = advance(state, i, j)
                total = total + abuf[j, 2 * heads + i:2 * heads + i + 1]
            stsend[d, h * HD:(h + 1) * HD] = state[0].astype(BF16)
            stsend[d, heads * HD + 16 * h:heads * HD + 16 * h + 16] = jnp.broadcast_to(state[1], (16, HD)).astype(BF16)
            scsend[d, h:h + 1] = state[2]
            scsend[d, heads + h:heads + h + 1] = total

    def state_copies(d, to):
        return (
            pltpu.make_async_remote_copy(
                src_ref=stsend.at[d], dst_ref=strecv.at[e], send_sem=s_send.at[to], recv_sem=s_recv.at[e],
                device_id=(to, t), device_id_type=MESH),
            pltpu.make_async_remote_copy(
                src_ref=scsend.at[d], dst_ref=screcv.at[e], send_sem=c_send.at[to], recv_sem=c_recv.at[e],
                device_id=(to, t), device_id_type=MESH),
        )

    def start_states(d):
        def one(to, carry):
            for c in state_copies(d, to):
                c.start()
            return carry
        return one

    lax.fori_loop(e + 1, E, start_states(0), 0)
    lax.fori_loop(0, e, start_states(1), 0)

    def forward(k):
        s = lax.rem(e - k + E, E)
        return pltpu.make_async_remote_copy(
            src_ref=xin.at[lo, s], dst_ref=xin.at[lo, s], send_sem=f_send.at[k], recv_sem=f_recv.at[k],
            device_id=(e, mate), device_id_type=MESH)

    own.wait()
    forward(0).start()

    def pass_on(k, carry):
        dispatch(k).wait_recv()
        forward(k).start()
        return carry

    lax.fori_loop(1, E, pass_on, 0)
    for i in range(5, 8):
        loads[H + i].wait()

    def give_half(k):
        s = lax.rem(e - k + E, E)
        return pltpu.make_async_remote_copy(
            src_ref=yboth.at[s, 1 - lo], dst_ref=yrecv.at[s], send_sem=y_send.at[k], recv_sem=y_recv.at[k],
            device_id=(e, mate), device_id_type=MESH)

    def give_back(k):
        s = lax.rem(e - k + E, E)
        return pltpu.make_async_remote_copy(
            src_ref=retsend.at[s], dst_ref=ret.at[e], send_sem=r_send.at[k], recv_sem=r_recv.at[k],
            device_id=(s, t), device_id_type=MESH)

    def finish(k):
        s = lax.rem(e - k + E, E)
        give_half(k).wait_recv()
        retsend[s] = (yboth[s, lo].astype(F32) + yrecv[s].astype(F32)).astype(BF16)
        give_back(k).start()

    def expert(k):
        s = lax.rem(e - k + E, E)
        forward(k).wait_recv()
        rows = xin[:, s].reshape(2 * R, D)
        gate = nn(rows, wgv[...])
        up = nn(rows, wuv[...])
        hid = (gate * jax.nn.sigmoid(gate) * up).astype(BF16)
        for c in range(0, D, CHUNK):
            y = nn(hid, wdv[:, c:c + CHUNK]).astype(BF16)
            yboth[s, :, :, c:c + CHUNK] = y.reshape(2, R, CHUNK)
        give_half(k).start()

    expert(1)

    def steps(k, carry):
        expert(k)
        finish(k - 1)
        return carry

    lax.fori_loop(2, E, steps, 0)
    expert(0)
    finish(E - 1)
    give_half(0).wait_recv()
    ret[e] = (yboth[e, lo].astype(F32) + yrecv[e].astype(F32)).astype(BF16)

    def wait_states(j, carry):
        pltpu.make_async_copy(strecv.at[j], strecv.at[j], s_recv.at[j]).wait()
        pltpu.make_async_copy(screcv.at[j], screcv.at[j], c_recv.at[j]).wait()
        return carry

    lax.fori_loop(0, e, wait_states, 0)
    lax.fori_loop(e + 1, E, wait_states, 0)

    def join(j, carry):
        out = []
        for h in range(heads):
            mem, nor, m = carry[3 * h:3 * h + 3]
            m_j = screcv[j, h:h + 1]
            base = m + screcv[j, heads + h:heads + h + 1]
            g = jnp.maximum(base, m_j)
            old, new = jnp.exp(base - g), jnp.exp(m_j - g)
            c_j = strecv[j, h * HD:(h + 1) * HD].astype(F32)
            n_j = strecv[j, heads * HD + 16 * h:heads * HD + 16 * h + 16].astype(F32)[0:1]
            out += [old * mem + new * c_j, old * nor + new * n_j, g]
        return tuple(out)

    zero = (jnp.zeros((HD, HD), F32), jnp.zeros((1, HD), F32), jnp.zeros((1, LANES), F32)) * heads
    for d in range(2):
        if d == 0:
            entry = lax.fori_loop(0, e, join, zero)
        else:
            entry = lax.fori_loop(0, E - 1 - e, lambda i, c: join(E - 1 - i, c), zero)
        for h in range(heads):
            i = d * heads + h
            state = entry[3 * h:3 * h + 3]
            for n, j in enumerate(order(d)):
                cin[j, i] = state[0].astype(BF16)
                nin[j, i:i + 1] = state[1]
                min_[j, i:i + 1] = state[2]
                if n < NB - 1:
                    state = advance(state, i, j)

    def mix(j, carry):
        at = pl.ds(pl.multiple_of(j * BLK, BLK), BLK)
        rows = rowsv[j]
        cols = colsv[j]
        for h in range(heads):
            hs = slice(h * HD, (h + 1) * HD)
            q, k, v = qs[at, hs], ks[at, hs], vs[at, hs]
            raw = nt(q, k)
            q_wide = q.astype(F32)
            both = None
            for d in range(2):
                i = d * heads + h
                mask = (pos_r >= pos_c) if d == 0 else (pos_r <= pos_c)
                a = jnp.where(mask, rows[i:i + 1], NEG)
                m_in = min_[j, i:i + 1][:, 0:1]
                g = jnp.maximum(jnp.max(a, axis=1, keepdims=True), m_in)
                s = raw * jnp.exp(a - g)
                w = jnp.exp(m_in - g)
                num = nn(s.astype(BF16), v) + w * nn(q, cin[j, i])
                den = jnp.sum(s, axis=1, keepdims=True) + w * jnp.sum(q_wide * nin[j, i:i + 1], axis=1, keepdims=True)
                floor = jnp.exp(-(cols[:, 2 * heads + i:2 * heads + i + 1] + g))
                part = num / jnp.maximum(jnp.abs(den), floor)
                both = part if both is None else both + part
            gated = jax.nn.sigmoid(os_[at, hs].astype(F32)) * both
            hsend[at, hs] = rms(gated, head_gain[:, hs]).astype(BF16)
        return carry

    lax.fori_loop(0, NB, mix, 0)
    MR = hsend.shape[0] // TP

    def share_h(k):
        to = lax.rem(t + k, TP)
        return pltpu.make_async_remote_copy(
            src_ref=hsend.at[pl.ds(pl.multiple_of(to * MR, MR), MR)], dst_ref=hrecv.at[t],
            send_sem=h_send.at[k], recv_sem=h_recv.at[k], device_id=(e, to), device_id_type=MESH)

    for k in range(1, TP):
        share_h(k).start()
    hrecv[t] = hsend[pl.ds(pl.multiple_of(t * MR, MR), MR), :]
    for k in range(1, TP):
        share_w(k).wait_recv()
        share_h(k).wait_recv()
    for c in range(0, D, CHUNK):
        acc = nn(hrecv[0], wfull[0, :, c:c + CHUNK])
        for g in range(1, TP):
            acc = acc + nn(hrecv[g], wfull[g, :, c:c + CHUNK])
        mixer_out[:, c:c + CHUNK] = acc.astype(BF16)

    for k in range(1, H):
        share_g(k).wait_recv()
    for k in range(1, E):
        give_back(k).wait_recv()

    def chosen(h):
        place = lax.broadcasted_iota(jnp.int32, (quarter, slots), 1)
        mat = None
        for j in range(TOPK):
            term = jnp.where(place == slot_v[h, j][:, 0:1], wts[h][:, j:j + 1], 0.0)
            mat = term if mat is None else mat + term
        return mat.astype(BF16)

    mats = [chosen(h) for h in range(H)]
    for h in range(H):
        for c in range(0, D, CHUNK):
            got = ret[:, h * cap:(h + 1) * cap, c:c + CHUNK].reshape(slots, CHUNK)
            outsend[h, :, c:c + CHUNK] = nn(mats[h], got).astype(BF16)

    def share_o(k):
        to = lax.rem(hi + k, H)
        return pltpu.make_async_remote_copy(
            src_ref=outsend.at[to], dst_ref=outrecv.at[hi], send_sem=o_send.at[k], recv_sem=o_recv.at[k],
            device_id=(e, 2 * to + lo), device_id_type=MESH)

    for k in range(1, H):
        share_o(k).start()
    total = outsend[hi].astype(F32)
    for k in range(1, H):
        share_o(k).wait_recv()
        total = total + outrecv[lax.rem(hi - k + H, H)].astype(F32)
    route_out[...] = total.astype(BF16)

    for k in range(1, E):
        dispatch(k).wait_send()
        give_back(k).wait_send()
    for k in range(E):
        forward(k).wait_send()
        give_half(k).wait_send()
    for k in range(1, TP):
        share_w(k).wait_send()
        share_h(k).wait_send()
    for k in range(1, H):
        share_g(k).wait_send()
        share_o(k).wait_send()

    def end_states(d):
        def one(to, carry):
            for c in state_copies(d, to):
                c.wait_send()
            return carry
        return one

    lax.fori_loop(e + 1, E, end_states(0), 0)
    lax.fori_loop(0, e, end_states(1), 0)


def shards(
    x_mix, mix_gain, w_query, w_key, w_value, w_outgate, w_gates, gate_bias, gate_drift,
    head_gain, w_out, x_route, route_gain, routes, route_weight, w_gate_e, w_up_e, w_down_e,
):
    E = lax.axis_size("ep")
    TP = lax.axis_size("tp")
    t = lax.axis_index("tp")
    rows, D = x_mix.shape
    width = w_query.shape[1]
    heads = width // HD
    NB = rows // BLK
    quarter = x_route.shape[0] // TP
    cap = 2 * quarter * TOPK // E
    H = TP // 2
    R = H * cap
    FH = w_gate_e.shape[2]
    MR = rows // TP
    own = lax.dynamic_slice_in_dim(w_gates.reshape(D, 4, -1), t * heads, heads, 2)
    gates_t = own.reshape(D, 4 * heads).T
    kind = jnp.arange(4, dtype=jnp.int32) % 2
    add = gate_bias[None] + gate_drift[:, None, None] * kind[None, :, None].astype(F32)
    add = jnp.broadcast_to(add.reshape(NB, 4 * heads, 1), (NB, 4 * heads, BLK))
    weights = jnp.pad(route_weight, ((0, 0), (0, LANES - TOPK)))
    anywhere = pl.BlockSpec(memory_space=pl.ANY)
    vmem = pl.BlockSpec(memory_space=pltpu.VMEM)
    V = pltpu.VMEM
    dma = pltpu.SemaphoreType.DMA
    SR = heads * HD + 16 * heads
    scratch = [
        V((rows, D), BF16), V((D, width), BF16), V((D, width), BF16), V((D, width), BF16), V((D, width), BF16),
        V((H, quarter, D), BF16), V((D, FH), BF16), V((D, FH), BF16), V((FH, D), BF16),
        V((TP, width, D), BF16), V((H, quarter, LANES), F32),
        V((E, R, D), BF16), V((2, E, R, D), BF16), V((E, 2, R, D), BF16), V((E, R, D), BF16),
        V((E, R, D), BF16), V((E, R, D), BF16), V((H, quarter, D), BF16), V((H, quarter, D), BF16),
        V((rows, width), BF16), V((rows, width), BF16), V((rows, width), BF16), V((rows, width), BF16),
        V((NB, 4 * heads, BLK), F32), V((NB, BLK, 4 * heads), F32), V((NB, 4 * heads, LANES), F32),
        V((NB, 2 * heads, HD, HD), F32), V((NB, 2 * heads, HD), F32),
        V((2, SR, HD), BF16), V((2, 8, LANES), F32), V((E, SR, HD), BF16), V((E, 8, LANES), F32),
        V((NB, 2 * heads, HD, HD), BF16), V((NB, 2 * heads, HD), F32), V((NB, 2 * heads, LANES), F32),
        V((rows, width), BF16), V((TP, MR, width), BF16), V((H, TOPK, quarter, LANES), jnp.int32),
        dma((H + 10,)), dma((1,)),
    ] + [dma((E,))] * 12 + [dma((TP,))] * 4 + [dma((H,))] * 4
    return pl.pallas_call(
        functools.partial(body, E, TP, heads, cap, quarter),
        out_shape=(jax.ShapeDtypeStruct((MR, D), BF16), jax.ShapeDtypeStruct((quarter, D), BF16)),
        in_specs=[anywhere] * 10 + [vmem] * 6 + [anywhere],
        out_specs=(vmem, vmem),
        scratch_shapes=scratch,
        compiler_params=pltpu.CompilerParams(
            collective_id=0, has_side_effects=True, vmem_limit_bytes=67043328),
    )(
        x_mix, w_query, w_key, w_value, w_outgate, x_route, w_gate_e[0], w_up_e[0], w_down_e[0], w_out,
        mix_gain[None], route_gain[None], head_gain[None], gates_t, add, routes, weights,
    )


def solution(mesh):
    return jax.shard_map(
        shards,
        mesh=mesh,
        in_specs=(
            P("ep", None), P(), P(None, "tp"), P(None, "tp"), P(None, "tp"), P(None, "tp"), P(),
            P(None, "tp"), P("ep"), P("tp"), P("tp", None), P("ep", None), P(), P("ep", None),
            P(("ep", "tp"), None), P("ep", None, "tp"), P("ep", None, "tp"), P("ep", "tp", None),
        ),
        out_specs=(P(("ep", "tp"), None), P(("ep", "tp"), None)),
        check_vma=False,
    )
```

profile of v0, /device:TPU:0, one launch (start us, length us, event | category | flops | bytes accessed | tf_op | source)
XLA Modules:
  0.0 256.5 jit_solution(5771463230942049903)
XLA Ops:
  0.6 0.7 broadcast_multiply_fusion
  1.4 0.8 copy.24
  2.1 0.1 add.37
  2.2 0.1 broadcast_add_fusion
  2.3 0.1 copy.25
  2.4 0.7 broadcast_in_dim.20.gate_add
  3.1 0.9 constant_dynamic-slice_fusion
  4.0 0.6 reshape.72
  4.6 0.8 copy.26
  5.4 0.6 pad.4.weights
  6.1 1.5 copy.27.routes
  7.6 244.7 %shard_map.185 = (bf16[256,2048]{1,0:T(8,128)(2,1)}, bf16[128,2048]{1,0:T(8,128)(2,1)}) custom-call(bf16[1024,2048]{1,0:T(8,128)(2,1)} %x_mix.1, bf16[2048,256]{1,0:T(8,128)(2,1)} %wq.1, bf16[2048,256]{1,0:T(8,128)(2,1)} %wk.1, bf16[2048,256]{1,0:T(8,128)(2,1)} %wv.1, bf16[2048,256]{1,0:T(8,128)(2,1)} %wo.1, bf16[512,2048]{1,0:T(8,128)(2,1)} %x_route.1, ...), custom_call_target="tpu_custom_call" | custom-call | tf_op jit(solution)/shard_map/pallas_call | solution.py:470
  252.3 2.3 copy.30
  254.6 1.9 copy.31
  (2 shorter events, 0.0 us)
where the time goes:
time: 257 us; the launch traced here: 256 us
  Pallas kernels  245 us (95%)
  local copies, waits for them, and re-layouts  10.3 us (4%)
    pallas_call x1, Pallas kernels, shards(): pl.pallas_call(functools.partial(body, E, TP, heads, cap, quarter), out_s...  245 us
    unnamed x5, local copies, waits for them, and re-layouts  7.27 us

commit v1 on v0

--- a/solution.py
+++ b/solution.py
@@ -41,34 +41,28 @@
     x_mix, wq, wk, wv, wo, x_route, wg_e, wu_e, wd_e, w_out,
     mix_gain, route_gain, head_gain, w_gates, gate_add, routes, weights,
     mixer_out, route_out,
-    xm, wqv, wkv, wvv, wov, xr, wgv, wuv, wdv, wfull, wts,
-    sendbuf, xin, yboth, yrecv, retsend, ret, outsend, outrecv,
+    xm, wqv, wkv, wvv, wov, xr, wgv, wuv, wdv, wfull,
+    sendbuf, xin, hid, retsend, ret,
     qs, ks, vs, os_, rowsv, colsv, abuf, kvb, nb, stsend, scsend, strecv, screcv,
     cin, nin, min_, hsend, hrecv, slot_v,
-    lsem, own_sem, d_send, d_recv, f_send, f_recv, y_send, y_recv, r_send, r_recv,
-    s_send, s_recv, c_send, c_recv, h_send, h_recv, w_send, w_recv, g_send, g_recv, o_send, o_recv,
+    lsem, own_sem, d_send, d_recv, r_send, r_recv,
+    s_send, s_recv, c_send, c_recv, h_send, h_recv, wx_send, wx_recv, wm_send, wm_recv,
 ):
     e = lax.axis_index("ep")
     t = lax.axis_index("tp")
     lo = lax.rem(t, 2)
-    hi = lax.div(t, 2)
     mate = t + 1 - 2 * lo
     H = TP // 2
-    R = H * cap
     D = xm.shape[1]
     NB = xm.shape[0] // BLK
     slots = E * cap
+    parts = ((wg_e, wgv), (wu_e, wuv), (wd_e, wdv), (w_out, wfull))
 
     loads = []
-    for h in range(H):
-        loads.append(pltpu.make_async_copy(
-            x_route.at[pl.ds((2 * h + lo) * quarter, quarter)], xr.at[h], lsem.at[h]))
     for i, (src, dst) in enumerate([
-        (x_mix, xm), (wq, wqv), (wk, wkv), (wv, wvv), (wo, wov),
-        (wg_e, wgv), (wu_e, wuv), (wd_e, wdv), (w_out, wfull.at[t]),
-    ]):
-        loads.append(pltpu.make_async_copy(src, dst, lsem.at[H + i]))
-    loads.append(pltpu.make_async_copy(weights, wts.at[hi], lsem.at[H + 9]))
+        (x_route.at[pl.ds(t * quarter, quarter)], xr), (x_mix, xm), (wq, wqv), (wk, wkv), (wv, wvv), (wo, wov),
+    ] + [(src, dst.at[t]) for src, dst in parts]):
+        loads.append(pltpu.make_async_copy(src, dst, lsem.at[i]))
     for c in loads:
         c.start()
 
@@ -79,58 +73,58 @@
         pl.semaphore_signal(barrier, inc=1, device_id=(e, lax.rem(t + k, TP)), device_id_type=MESH)
     pl.semaphore_wait(barrier, E - 1 + TP - 1)
 
+    def across(i, k):
+        src, dst = parts[i]
+        return pltpu.make_async_remote_copy(
+            src_ref=src, dst_ref=dst.at[t], send_sem=wx_send.at[i, k], recv_sem=wx_recv.at[i, k],
+            device_id=(e, lax.rem(t + 2 * k, TP)), device_id_type=MESH)
+
+    def to_mate(i, k):
+        src, dst = parts[i]
+        whose = lax.rem(t - 2 * k + TP, TP)
+        return pltpu.make_async_remote_copy(
+            src_ref=src if k == 0 else dst.at[whose], dst_ref=dst.at[whose],
+            send_sem=wm_send.at[i, k], recv_sem=wm_recv.at[i, k], device_id=(e, mate), device_id_type=MESH)
+
+    for i in range(4):
+        for k in range(1, H):
+            across(i, k).start()
+
     tri = (lax.broadcasted_iota(jnp.int32, (quarter, quarter), 0)
            > lax.broadcasted_iota(jnp.int32, (quarter, quarter), 1)).astype(BF16)
-    for h in range(H):
-        loads[h].wait()
-        rows = rms(xr[h], route_gain[...]).astype(BF16)
-        table = routes[pl.ds((2 * h + lo) * quarter, quarter), :]
-        experts = lax.broadcasted_iota(jnp.int32, (quarter, E), 1)
-        hot = [(experts == table[:, j:j + 1]).astype(F32) for j in range(TOPK)]
-        before = nn(tri, sum(hot).astype(BF16))
-        place = lax.broadcasted_iota(jnp.int32, (quarter, slots), 1)
-        pick = None
-        for j in range(TOPK):
-            slot = table[:, j:j + 1] * cap + jnp.sum(before * hot[j], axis=1, keepdims=True).astype(jnp.int32)
-            slot_v[h, j] = jnp.broadcast_to(slot, (quarter, LANES))
-            here = (place == slot).astype(F32)
-            pick = here if pick is None else pick + here
-        pick = pick.astype(BF16)
-        for c in range(0, D, CHUNK):
-            packed = tn(pick, rows[:, c:c + CHUNK]).astype(BF16)
-            sendbuf[:, h * cap:(h + 1) * cap, c:c + CHUNK] = packed.reshape(E, cap, CHUNK)
+    loads[0].wait()
+    table = routes[pl.ds(t * quarter, quarter), :]
+    experts = lax.broadcasted_iota(jnp.int32, (quarter, E), 1)
+    hot = [(experts == table[:, j:j + 1]).astype(F32) for j in range(TOPK)]
+    before = nn(tri, sum(hot).astype(BF16))
+    place = lax.broadcasted_iota(jnp.int32, (quarter, slots), 1)
+    pick = None
+    for j in range(TOPK):
+        slot = table[:, j:j + 1] * cap + jnp.sum(before * hot[j], axis=1, keepdims=True).astype(jnp.int32)
+        slot_v[j] = jnp.broadcast_to(slot, (quarter, LANES))
+        here = (place == slot).astype(F32)
+        pick = here if pick is None else pick + here
+    pick = pick.astype(BF16)
+    normed_rows = rms(xr[...], route_gain[...]).astype(BF16)
+    for c in range(0, D, CHUNK):
+        packed = tn(pick, normed_rows[:, c:c + CHUNK]).astype(BF16)
+        sendbuf[:, :, c:c + CHUNK] = packed.reshape(E, cap, CHUNK)
 
     def dispatch(k):
         to = lax.rem(e + k, E)
         return pltpu.make_async_remote_copy(
-            src_ref=sendbuf.at[to], dst_ref=xin.at[lo, e], send_sem=d_send.at[k], recv_sem=d_recv.at[k],
+            src_ref=sendbuf.at[to], dst_ref=xin.at[e], send_sem=d_send.at[k], recv_sem=d_recv.at[k],
             device_id=(to, t), device_id_type=MESH)
 
-    own = pltpu.make_async_copy(sendbuf.at[e], xin.at[lo, e], own_sem.at[0])
+    own = pltpu.make_async_copy(sendbuf.at[e], xin.at[e], own_sem.at[0])
     own.start()
     for k in range(1, E):
         dispatch(k).start()
-
-    loads[H + 8].wait()
-    loads[H + 9].wait()
-
-    def share_w(k):
-        return pltpu.make_async_remote_copy(
-            src_ref=wfull.at[t], dst_ref=wfull.at[t], send_sem=w_send.at[k], recv_sem=w_recv.at[k],
-            device_id=(e, lax.rem(t + k, TP)), device_id_type=MESH)
-
-    def share_g(k):
-        return pltpu.make_async_remote_copy(
-            src_ref=wts.at[hi], dst_ref=wts.at[hi], send_sem=g_send.at[k], recv_sem=g_recv.at[k],
-            device_id=(e, lax.rem(t + 2 * k, TP)), device_id_type=MESH)
-
-    for k in range(1, H):
-        share_g(k).start()
-    for k in range(1, TP):
-        share_w(k).start()
-
-    for i in range(5):
-        loads[H + i].wait()
+    for i in range(4):
+        to_mate(i, 0).start()
+
+    for i in range(1, 6):
+        loads[i].wait()
     pos_r = lax.broadcasted_iota(jnp.int32, (BLK, BLK), 0)
     pos_c = lax.broadcasted_iota(jnp.int32, (BLK, BLK), 1)
 
@@ -222,66 +216,30 @@
     lax.fori_loop(e + 1, E, start_states(0), 0)
     lax.fori_loop(0, e, start_states(1), 0)
 
-    def forward(k):
-        s = lax.rem(e - k + E, E)
-        return pltpu.make_async_remote_copy(
-            src_ref=xin.at[lo, s], dst_ref=xin.at[lo, s], send_sem=f_send.at[k], recv_sem=f_recv.at[k],
-            device_id=(e, mate), device_id_type=MESH)
-
     own.wait()
-    forward(0).start()
-
-    def pass_on(k, carry):
+    for k in range(1, E):
         dispatch(k).wait_recv()
-        forward(k).start()
-        return carry
-
-    lax.fori_loop(1, E, pass_on, 0)
-    for i in range(5, 8):
-        loads[H + i].wait()
-
-    def give_half(k):
-        s = lax.rem(e - k + E, E)
-        return pltpu.make_async_remote_copy(
-            src_ref=yboth.at[s, 1 - lo], dst_ref=yrecv.at[s], send_sem=y_send.at[k], recv_sem=y_recv.at[k],
-            device_id=(e, mate), device_id_type=MESH)
-
-    def give_back(k):
-        s = lax.rem(e - k + E, E)
-        return pltpu.make_async_remote_copy(
-            src_ref=retsend.at[s], dst_ref=ret.at[e], send_sem=r_send.at[k], recv_sem=r_recv.at[k],
-            device_id=(s, t), device_id_type=MESH)
-
-    def finish(k):
-        s = lax.rem(e - k + E, E)
-        give_half(k).wait_recv()
-        retsend[s] = (yboth[s, lo].astype(F32) + yrecv[s].astype(F32)).astype(BF16)
-        give_back(k).start()
-
-    def expert(k):
-        s = lax.rem(e - k + E, E)
-        forward(k).wait_recv()
-        rows = xin[:, s].reshape(2 * R, D)
-        gate = nn(rows, wgv[...])
-        up = nn(rows, wuv[...])
-        hid = (gate * jax.nn.sigmoid(gate) * up).astype(BF16)
-        for c in range(0, D, CHUNK):
-            y = nn(hid, wdv[:, c:c + CHUNK]).astype(BF16)
-            yboth[s, :, :, c:c + CHUNK] = y.reshape(2, R, CHUNK)
-        give_half(k).start()
-
-    expert(1)
-
-    def steps(k, carry):
-        expert(k)
-        finish(k - 1)
-        return carry
-
-    lax.fori_loop(2, E, steps, 0)
-    expert(0)
-    finish(E - 1)
-    give_half(0).wait_recv()
-    ret[e] = (yboth[e, lo].astype(F32) + yrecv[e].astype(F32)).astype(BF16)
+
+    def hidden(g):
+        rows = xin[...].reshape(slots, D)
+        gate = nn(rows, wgv[g])
+        up = nn(rows, wuv[g])
+        hid[g] = (gate * jax.nn.sigmoid(gate) * up).astype(BF16)
+
+    for i in range(6, 10):
+        loads[i].wait()
+    hidden(t)
+    for i in range(2):
+        to_mate(i, 0).wait_recv()
+    hidden(mate)
+    for k in range(1, H):
+        for i in range(2):
+            across(i, k).wait_recv()
+            to_mate(i, k).start()
+        hidden(lax.rem(t - 2 * k + TP, TP))
+        for i in range(2):
+            to_mate(i, k).wait_recv()
+        hidden(lax.rem(mate - 2 * k + TP, TP))
 
     def wait_states(j, carry):
         pltpu.make_async_copy(strecv.at[j], strecv.at[j], s_recv.at[j]).wait()
@@ -359,8 +317,44 @@
     for k in range(1, TP):
         share_h(k).start()
     hrecv[t] = hsend[pl.ds(pl.multiple_of(t * MR, MR), MR), :]
+
+    for k in range(1, H):
+        across(2, k).wait_recv()
+        to_mate(2, k).start()
+    for k in range(H):
+        to_mate(2, k).wait_recv()
+
+    def give_back(k):
+        s = lax.rem(e + k, E)
+        return pltpu.make_async_remote_copy(
+            src_ref=retsend.at[s], dst_ref=ret.at[e], send_sem=r_send.at[k], recv_sem=r_recv.at[k],
+            device_id=(s, t), device_id_type=MESH)
+
+    group = max(1, 2 * LANES // cap)
+    span = group * cap
+    for n in range(E // group):
+        first = lax.rem(e // group + n + 1, E // group)
+        at = pl.ds(pl.multiple_of(first * span, span), span)
+        for c in range(0, D, CHUNK):
+            y = nn(hid[0, at, :], wdv[0, :, c:c + CHUNK])
+            for g in range(1, TP):
+                y = y + nn(hid[g, at, :], wdv[g, :, c:c + CHUNK])
+            retsend[pl.ds(first * group, group), :, c:c + CHUNK] = y.astype(BF16).reshape(group, cap, CHUNK)
+        for m in range(group):
+            s = first * group + m
+
+            @pl.when(s != e)
+            def _():
+                give_back(lax.rem(s - e + E, E)).start()
+
+    ret[e] = retsend[e]
+
+    for k in range(1, H):
+        across(3, k).wait_recv()
+        to_mate(3, k).start()
+    for k in range(H):
+        to_mate(3, k).wait_recv()
     for k in range(1, TP):
-        share_w(k).wait_recv()
         share_h(k).wait_recv()
     for c in range(0, D, CHUNK):
         acc = nn(hrecv[0], wfull[0, :, c:c + CHUNK])
@@ -368,51 +362,27 @@
             acc = acc + nn(hrecv[g], wfull[g, :, c:c + CHUNK])
         mixer_out[:, c:c + CHUNK] = acc.astype(BF16)
 
-    for k in range(1, H):
-        share_g(k).wait_recv()
     for k in range(1, E):
         give_back(k).wait_recv()
-
-    def chosen(h):
-        place = lax.broadcasted_iota(jnp.int32, (quarter, slots), 1)
-        mat = None
-        for j in range(TOPK):
-            term = jnp.where(place == slot_v[h, j][:, 0:1], wts[h][:, j:j + 1], 0.0)
-            mat = term if mat is None else mat + term
-        return mat.astype(BF16)
-
-    mats = [chosen(h) for h in range(H)]
-    for h in range(H):
-        for c in range(0, D, CHUNK):
-            got = ret[:, h * cap:(h + 1) * cap, c:c + CHUNK].reshape(slots, CHUNK)
-            outsend[h, :, c:c + CHUNK] = nn(mats[h], got).astype(BF16)
-
-    def share_o(k):
-        to = lax.rem(hi + k, H)
-        return pltpu.make_async_remote_copy(
-            src_ref=outsend.at[to], dst_ref=outrecv.at[hi], send_sem=o_send.at[k], recv_sem=o_recv.at[k],
-            device_id=(e, 2 * to + lo), device_id_type=MESH)
-
-    for k in range(1, H):
-        share_o(k).start()
-    total = outsend[hi].astype(F32)
-    for k in range(1, H):
-        share_o(k).wait_recv()
-        total = total + outrecv[lax.rem(hi - k + H, H)].astype(F32)
-    route_out[...] = total.astype(BF16)
+    mat = None
+    for j in range(TOPK):
+        term = jnp.where(place == slot_v[j][:, 0:1], weights[:, j:j + 1], 0.0)
+        mat = term if mat is None else mat + term
+    mat = mat.astype(BF16)
+    for c in range(0, D, CHUNK):
+        got = ret[:, :, c:c + CHUNK].reshape(slots, CHUNK)
+        route_out[:, c:c + CHUNK] = nn(mat, got).astype(BF16)
 
     for k in range(1, E):
         dispatch(k).wait_send()
         give_back(k).wait_send()
-    for k in range(E):
-        forward(k).wait_send()
-        give_half(k).wait_send()
+    for i in range(4):
+        for k in range(1, H):
+            across(i, k).wait_send()
+        for k in range(H):
+            to_mate(i, k).wait_send()
     for k in range(1, TP):
-        share_w(k).wait_send()
         share_h(k).wait_send()
-    for k in range(1, H):
-        share_g(k).wait_send()
-        share_o(k).wait_send()
 
     def end_states(d):
         def one(to, carry):
@@ -439,7 +409,6 @@
     quarter = x_route.shape[0] // TP
     cap = 2 * quarter * TOPK // E
     H = TP // 2
-    R = H * cap
     FH = w_gate_e.shape[2]
     MR = rows // TP
     own = lax.dynamic_slice_in_dim(w_gates.reshape(D, 4, -1), t * heads, heads, 2)
@@ -447,7 +416,6 @@
     kind = jnp.arange(4, dtype=jnp.int32) % 2
     add = gate_bias[None] + gate_drift[:, None, None] * kind[None, :, None].astype(F32)
     add = jnp.broadcast_to(add.reshape(NB, 4 * heads, 1), (NB, 4 * heads, BLK))
-    weights = jnp.pad(route_weight, ((0, 0), (0, LANES - TOPK)))
     anywhere = pl.BlockSpec(memory_space=pl.ANY)
     vmem = pl.BlockSpec(memory_space=pltpu.VMEM)
     V = pltpu.VMEM
@@ -455,29 +423,29 @@
     SR = heads * HD + 16 * heads
     scratch = [
         V((rows, D), BF16), V((D, width), BF16), V((D, width), BF16), V((D, width), BF16), V((D, width), BF16),
-        V((H, quarter, D), BF16), V((D, FH), BF16), V((D, FH), BF16), V((FH, D), BF16),
-        V((TP, width, D), BF16), V((H, quarter, LANES), F32),
-        V((E, R, D), BF16), V((2, E, R, D), BF16), V((E, 2, R, D), BF16), V((E, R, D), BF16),
-        V((E, R, D), BF16), V((E, R, D), BF16), V((H, quarter, D), BF16), V((H, quarter, D), BF16),
+        V((quarter, D), BF16), V((TP, D, FH), BF16), V((TP, D, FH), BF16), V((TP, FH, D), BF16),
+        V((TP, width, D), BF16),
+        V((E, cap, D), BF16), V((E, cap, D), BF16), V((TP, E * cap, FH), BF16), V((E, cap, D), BF16),
+        V((E, cap, D), BF16),
         V((rows, width), BF16), V((rows, width), BF16), V((rows, width), BF16), V((rows, width), BF16),
         V((NB, 4 * heads, BLK), F32), V((NB, BLK, 4 * heads), F32), V((NB, 4 * heads, LANES), F32),
         V((NB, 2 * heads, HD, HD), F32), V((NB, 2 * heads, HD), F32),
         V((2, SR, HD), BF16), V((2, 8, LANES), F32), V((E, SR, HD), BF16), V((E, 8, LANES), F32),
         V((NB, 2 * heads, HD, HD), BF16), V((NB, 2 * heads, HD), F32), V((NB, 2 * heads, LANES), F32),
-        V((rows, width), BF16), V((TP, MR, width), BF16), V((H, TOPK, quarter, LANES), jnp.int32),
-        dma((H + 10,)), dma((1,)),
-    ] + [dma((E,))] * 12 + [dma((TP,))] * 4 + [dma((H,))] * 4
+        V((rows, width), BF16), V((TP, MR, width), BF16), V((TOPK, quarter, LANES), jnp.int32),
+        dma((10,)), dma((1,)),
+    ] + [dma((E,))] * 8 + [dma((TP,))] * 2 + [dma((4, H))] * 4
     return pl.pallas_call(
         functools.partial(body, E, TP, heads, cap, quarter),
         out_shape=(jax.ShapeDtypeStruct((MR, D), BF16), jax.ShapeDtypeStruct((quarter, D), BF16)),
-        in_specs=[anywhere] * 10 + [vmem] * 6 + [anywhere],
+        in_specs=[anywhere] * 10 + [vmem] * 7,
         out_specs=(vmem, vmem),
         scratch_shapes=scratch,
         compiler_params=pltpu.CompilerParams(
             collective_id=0, has_side_effects=True, vmem_limit_bytes=67043328),
     )(
         x_mix, w_query, w_key, w_value, w_outgate, x_route, w_gate_e[0], w_up_e[0], w_down_e[0], w_out,
-        mix_gain[None], route_gain[None], head_gain[None], gates_t, add, routes, weights,
+        mix_gain[None], route_gain[None], head_gain[None], gates_t, add, routes, route_weight,
     )
 
 

time: 257 us -> 142 us (0.55)
  the two profiles are of different devices: /device:TPU:0 before, /device:TPU:31 now
where the time goes in v1:
time: 142 us
  Pallas kernels  130 us (92%)
  local copies, waits for them, and re-layouts  10.3 us (7%)
    pallas_call x1, Pallas kernels, shards(): pl.pallas_call(functools.partial(body, E, TP, heads, cap, quarter), out_s...  130 us
    unnamed x5, local copies, waits for them, and re-layouts  7.9 us

profile of v1, /device:TPU:31, one launch (start us, length us, event | category | flops | bytes accessed | tf_op | source)
XLA Modules:
  0.0 141.9 jit_solution(8826042365904046674)
XLA Ops:
  0.6 0.7 broadcast_multiply_fusion
  1.4 0.8 copy.24
  2.1 0.1 add.35
  2.2 0.1 broadcast_add_fusion
  2.3 0.1 copy.25
  2.4 0.7 broadcast_in_dim.20.gate_add
  3.1 0.9 constant_dynamic-slice_fusion
  4.0 0.6 reshape.72
  4.6 1.4 copy.27.weights
  6.0 1.5 %copy.26.routes = s32[512,2]{1,0:T(8,128)} copy(s32[512,2]{0,1:T(2,128)} %param.31) | data formatting | bytes 8192 | tf_op args[13]
  7.6 130.1 %shard_map.185 = (bf16[256,2048]{1,0:T(8,128)(2,1)}, bf16[128,2048]{1,0:T(8,128)(2,1)}) custom-call(bf16[1024,2048]{1,0:T(8,128)(2,1)} %x_mix.1, bf16[2048,256]{1,0:T(8,128)(2,1)} %wq.1, bf16[2048,256]{1,0:T(8,128)(2,1)} %wk.1, bf16[2048,256]{1,0:T(8,128)(2,1)} %wv.1, bf16[2048,256]{1,0:T(8,128)(2,1)} %wo.1, bf16[512,2048]{1,0:T(8,128)(2,1)} %x_route.1, ...), custom_call_target="tpu_custom_call" | custom-call | tf_op jit(solution)/shard_map/pallas_call | solution.py:438
  137.7 2.3 %copy.30 = bf16[256,2048]{1,0:T(8,128)(2,1)} copy(bf16[256,2048]{1,0:T(8,128)(2,1)} %get-tuple-element.4) | data formatting | bytes 2097152
  140.0 1.9 %copy.31 = bf16[128,2048]{1,0:T(8,128)(2,1)} copy(bf16[128,2048]{1,0:T(8,128)(2,1)} %get-tuple-element.5) | data formatting | bytes 1048576
  (2 shorter events, 0.0 us)

commit v2 on v1

--- a/solution.py
+++ b/solution.py
@@ -39,12 +39,12 @@
 def body(
     E, TP, heads, cap, quarter,
     x_mix, wq, wk, wv, wo, x_route, wg_e, wu_e, wd_e, w_out,
-    mix_gain, route_gain, head_gain, w_gates, gate_add, routes, weights,
+    mix_gain, route_gain, head_gain, w_gates, gate_bias, gate_drift, routes, weights,
     mixer_out, route_out,
     xm, wqv, wkv, wvv, wov, xr, wgv, wuv, wdv, wfull,
     sendbuf, xin, hid, retsend, ret,
     qs, ks, vs, os_, rowsv, colsv, abuf, kvb, nb, stsend, scsend, strecv, screcv,
-    cin, nin, min_, hsend, hrecv, slot_v,
+    cin, nin, min_, hsend, hrecv, slot_v, gate_add, gate_w,
     lsem, own_sem, d_send, d_recv, r_send, r_recv,
     s_send, s_recv, c_send, c_recv, h_send, h_recv, wx_send, wx_recv, wm_send, wm_recv,
 ):
@@ -56,7 +56,14 @@
     D = xm.shape[1]
     NB = xm.shape[0] // BLK
     slots = E * cap
-    parts = ((wg_e, wgv), (wu_e, wuv), (wd_e, wdv), (w_out, wfull))
+    half = wd_e.shape[0] // 2
+    parts = (
+        (wg_e, wgv), (wu_e, wuv),
+        (wd_e.at[pl.ds(0, half)], wdv.at[:, pl.ds(0, half)]),
+        (wd_e.at[pl.ds(half, half)], wdv.at[:, pl.ds(half, half)]),
+        (w_out, wfull),
+    )
+    n_parts = len(parts)
 
     loads = []
     for i, (src, dst) in enumerate([
@@ -86,28 +93,28 @@
             src_ref=src if k == 0 else dst.at[whose], dst_ref=dst.at[whose],
             send_sem=wm_send.at[i, k], recv_sem=wm_recv.at[i, k], device_id=(e, mate), device_id_type=MESH)
 
-    for i in range(4):
+    for i in range(n_parts):
         for k in range(1, H):
             across(i, k).start()
 
     tri = (lax.broadcasted_iota(jnp.int32, (quarter, quarter), 0)
-           > lax.broadcasted_iota(jnp.int32, (quarter, quarter), 1)).astype(BF16)
+           < lax.broadcasted_iota(jnp.int32, (quarter, quarter), 1)).astype(BF16)
     loads[0].wait()
-    table = routes[pl.ds(t * quarter, quarter), :]
-    experts = lax.broadcasted_iota(jnp.int32, (quarter, E), 1)
-    hot = [(experts == table[:, j:j + 1]).astype(F32) for j in range(TOPK)]
-    before = nn(tri, sum(hot).astype(BF16))
-    place = lax.broadcasted_iota(jnp.int32, (quarter, slots), 1)
+    place = lax.broadcasted_iota(jnp.int32, (slots, quarter), 0)
+    experts = lax.broadcasted_iota(jnp.int32, (E, quarter), 0)
+    table = routes[:, pl.ds(pl.multiple_of(t * quarter, quarter), quarter)]
+    hot = [(experts == table[j:j + 1]).astype(F32) for j in range(TOPK)]
+    before = nn(sum(hot).astype(BF16), tri)
     pick = None
     for j in range(TOPK):
-        slot = table[:, j:j + 1] * cap + jnp.sum(before * hot[j], axis=1, keepdims=True).astype(jnp.int32)
-        slot_v[j] = jnp.broadcast_to(slot, (quarter, LANES))
+        slot = table[j:j + 1] * cap + jnp.sum(before * hot[j], axis=0, keepdims=True).astype(jnp.int32)
+        slot_v[j:j + 1] = slot
         here = (place == slot).astype(F32)
         pick = here if pick is None else pick + here
     pick = pick.astype(BF16)
     normed_rows = rms(xr[...], route_gain[...]).astype(BF16)
     for c in range(0, D, CHUNK):
-        packed = tn(pick, normed_rows[:, c:c + CHUNK]).astype(BF16)
+        packed = nn(pick, normed_rows[:, c:c + CHUNK]).astype(BF16)
         sendbuf[:, :, c:c + CHUNK] = packed.reshape(E, cap, CHUNK)
 
     def dispatch(k):
@@ -120,13 +127,30 @@
     own.start()
     for k in range(1, E):
         dispatch(k).start()
-    for i in range(4):
+    for i in range(n_parts):
         to_mate(i, 0).start()
 
     for i in range(1, 6):
         loads[i].wait()
     pos_r = lax.broadcasted_iota(jnp.int32, (BLK, BLK), 0)
     pos_c = lax.broadcasted_iota(jnp.int32, (BLK, BLK), 1)
+
+    width = w_gates.shape[0] // 4
+    row = lax.broadcasted_iota(jnp.int32, (4 * heads, 4 * width), 0)
+    col = lax.broadcasted_iota(jnp.int32, (4 * heads, 4 * width), 1)
+    own_rows = None
+    for g in range(4):
+        for h in range(heads):
+            here = ((row == g * heads + h) & (col == g * width + t * heads + h)).astype(F32)
+            own_rows = here if own_rows is None else own_rows + here
+    gate_w[...] = nn(own_rows.astype(BF16), w_gates[...]).astype(BF16)
+    for j in range(NB):
+        for g in range(4):
+            for h in range(heads):
+                value = gate_bias[h:h + 1, g:g + 1]
+                if g % 2 == 1:
+                    value = value + gate_drift[:, j:j + 1]
+                gate_add[j, g * heads + h:g * heads + h + 1] = jnp.broadcast_to(value, (1, BLK))
 
     def project(j, carry):
         at = pl.ds(pl.multiple_of(j * BLK, BLK), BLK)
@@ -137,7 +161,7 @@
         ks[at, :] = k_all
         vs[at, :] = v_all
         os_[at, :] = nn(normed, wov[...]).astype(BF16)
-        pre = nt(w_gates[...], normed) + gate_add[j]
+        pre = nt(gate_w[...], normed) + gate_add[j]
         logf = jnp.minimum(pre, 0.0) - jnp.log1p(jnp.exp(-jnp.abs(pre)))
         upper = (pos_r <= pos_c).astype(F32)
         lower = (pos_r >= pos_c).astype(F32)
@@ -226,7 +250,7 @@
         up = nn(rows, wuv[g])
         hid[g] = (gate * jax.nn.sigmoid(gate) * up).astype(BF16)
 
-    for i in range(6, 10):
+    for i in range(6, 6 + n_parts):
         loads[i].wait()
     hidden(t)
     for i in range(2):
@@ -240,6 +264,39 @@
         for i in range(2):
             to_mate(i, k).wait_recv()
         hidden(lax.rem(mate - 2 * k + TP, TP))
+
+    for i in (2, 3):
+        for k in range(1, H):
+            across(i, k).wait_recv()
+            to_mate(i, k).start()
+    for i in (2, 3):
+        for k in range(H):
+            to_mate(i, k).wait_recv()
+
+    def give_back(k):
+        s = lax.rem(e + k, E)
+        return pltpu.make_async_remote_copy(
+            src_ref=retsend.at[s], dst_ref=ret.at[e], send_sem=r_send.at[k], recv_sem=r_recv.at[k],
+            device_id=(s, t), device_id_type=MESH)
+
+    group = max(1, 2 * LANES // cap)
+    span = group * cap
+    for n in range(E // group):
+        first = lax.rem(e // group + n + 1, E // group)
+        at = pl.ds(pl.multiple_of(first * span, span), span)
+        for c in range(0, D, CHUNK):
+            y = nn(hid[0, at, :], wdv[0, :, c:c + CHUNK])
+            for g in range(1, TP):
+                y = y + nn(hid[g, at, :], wdv[g, :, c:c + CHUNK])
+            retsend[pl.ds(first * group, group), :, c:c + CHUNK] = y.astype(BF16).reshape(group, cap, CHUNK)
+        for m in range(group):
+            s = first * group + m
+
+            @pl.when(s != e)
+            def _():
+                give_back(lax.rem(s - e + E, E)).start()
+
+    ret[e] = retsend[e]
 
     def wait_states(j, carry):
         pltpu.make_async_copy(strecv.at[j], strecv.at[j], s_recv.at[j]).wait()
@@ -319,41 +376,10 @@
     hrecv[t] = hsend[pl.ds(pl.multiple_of(t * MR, MR), MR), :]
 
     for k in range(1, H):
-        across(2, k).wait_recv()
-        to_mate(2, k).start()
+        across(4, k).wait_recv()
+        to_mate(4, k).start()
     for k in range(H):
-        to_mate(2, k).wait_recv()
-
-    def give_back(k):
-        s = lax.rem(e + k, E)
-        return pltpu.make_async_remote_copy(
-            src_ref=retsend.at[s], dst_ref=ret.at[e], send_sem=r_send.at[k], recv_sem=r_recv.at[k],
-            device_id=(s, t), device_id_type=MESH)
-
-    group = max(1, 2 * LANES // cap)
-    span = group * cap
-    for n in range(E // group):
-        first = lax.rem(e // group + n + 1, E // group)
-        at = pl.ds(pl.multiple_of(first * span, span), span)
-        for c in range(0, D, CHUNK):
-            y = nn(hid[0, at, :], wdv[0, :, c:c + CHUNK])
-            for g in range(1, TP):
-                y = y + nn(hid[g, at, :], wdv[g, :, c:c + CHUNK])
-            retsend[pl.ds(first * group, group), :, c:c + CHUNK] = y.astype(BF16).reshape(group, cap, CHUNK)
-        for m in range(group):
-            s = first * group + m
-
-            @pl.when(s != e)
-            def _():
-                give_back(lax.rem(s - e + E, E)).start()
-
-    ret[e] = retsend[e]
-
-    for k in range(1, H):
-        across(3, k).wait_recv()
-        to_mate(3, k).start()
-    for k in range(H):
-        to_mate(3, k).wait_recv()
+        to_mate(4, k).wait_recv()
     for k in range(1, TP):
         share_h(k).wait_recv()
     for c in range(0, D, CHUNK):
@@ -366,17 +392,17 @@
         give_back(k).wait_recv()
     mat = None
     for j in range(TOPK):
-        term = jnp.where(place == slot_v[j][:, 0:1], weights[:, j:j + 1], 0.0)
+        term = jnp.where(place == slot_v[j:j + 1], weights[j:j + 1], 0.0)
         mat = term if mat is None else mat + term
     mat = mat.astype(BF16)
     for c in range(0, D, CHUNK):
         got = ret[:, :, c:c + CHUNK].reshape(slots, CHUNK)
-        route_out[:, c:c + CHUNK] = nn(mat, got).astype(BF16)
+        route_out[:, c:c + CHUNK] = tn(mat, got).astype(BF16)
 
     for k in range(1, E):
         dispatch(k).wait_send()
         give_back(k).wait_send()
-    for i in range(4):
+    for i in range(n_parts):
         for k in range(1, H):
             across(i, k).wait_send()
         for k in range(H):
@@ -401,7 +427,6 @@
 ):
     E = lax.axis_size("ep")
     TP = lax.axis_size("tp")
-    t = lax.axis_index("tp")
     rows, D = x_mix.shape
     width = w_query.shape[1]
     heads = width // HD
@@ -411,11 +436,6 @@
     H = TP // 2
     FH = w_gate_e.shape[2]
     MR = rows // TP
-    own = lax.dynamic_slice_in_dim(w_gates.reshape(D, 4, -1), t * heads, heads, 2)
-    gates_t = own.reshape(D, 4 * heads).T
-    kind = jnp.arange(4, dtype=jnp.int32) % 2
-    add = gate_bias[None] + gate_drift[:, None, None] * kind[None, :, None].astype(F32)
-    add = jnp.broadcast_to(add.reshape(NB, 4 * heads, 1), (NB, 4 * heads, BLK))
     anywhere = pl.BlockSpec(memory_space=pl.ANY)
     vmem = pl.BlockSpec(memory_space=pltpu.VMEM)
     V = pltpu.VMEM
@@ -432,20 +452,21 @@
         V((NB, 2 * heads, HD, HD), F32), V((NB, 2 * heads, HD), F32),
         V((2, SR, HD), BF16), V((2, 8, LANES), F32), V((E, SR, HD), BF16), V((E, 8, LANES), F32),
         V((NB, 2 * heads, HD, HD), BF16), V((NB, 2 * heads, HD), F32), V((NB, 2 * heads, LANES), F32),
-        V((rows, width), BF16), V((TP, MR, width), BF16), V((TOPK, quarter, LANES), jnp.int32),
-        dma((10,)), dma((1,)),
-    ] + [dma((E,))] * 8 + [dma((TP,))] * 2 + [dma((4, H))] * 4
+        V((rows, width), BF16), V((TP, MR, width), BF16), V((TOPK, quarter), jnp.int32), V((NB, 4 * heads, BLK), F32), V((4 * heads, D), BF16),
+        dma((11,)), dma((1,)),
+    ] + [dma((E,))] * 8 + [dma((TP,))] * 2 + [dma((5, H))] * 4
     return pl.pallas_call(
         functools.partial(body, E, TP, heads, cap, quarter),
         out_shape=(jax.ShapeDtypeStruct((MR, D), BF16), jax.ShapeDtypeStruct((quarter, D), BF16)),
-        in_specs=[anywhere] * 10 + [vmem] * 7,
+        in_specs=[anywhere] * 10 + [vmem] * 8,
         out_specs=(vmem, vmem),
         scratch_shapes=scratch,
         compiler_params=pltpu.CompilerParams(
             collective_id=0, has_side_effects=True, vmem_limit_bytes=67043328),
     )(
         x_mix, w_query, w_key, w_value, w_outgate, x_route, w_gate_e[0], w_up_e[0], w_down_e[0], w_out,
-        mix_gain[None], route_gain[None], head_gain[None], gates_t, add, routes, route_weight,
+        mix_gain[None], route_gain[None], head_gain[None], w_gates.T, gate_bias.T, gate_drift[None], routes.T,
+        route_weight.T,
     )
 
 

time: 142 us -> 134 us (0.944)
  the two profiles are of different devices: /device:TPU:31 before, /device:TPU:29 now
where the time goes in v2:
time: 134 us
  Pallas kernels  129 us (96%)
  local copies, waits for them, and re-layouts  4.18 us (3%)
    pallas_call x1, Pallas kernels, shards(): pl.pallas_call(functools.partial(body, E, TP, heads, cap, quarter), out_s...  129 us
    unnamed x2, local copies, waits for them, and re-layouts  4.18 us

profile of v2, /device:TPU:29, one launch (start us, length us, event | category | flops | bytes accessed | tf_op | source)
XLA Modules:
  0.0 133.8 jit_solution(6812434641033448579)
XLA Ops:
  0.6 128.9 %shard_map.185 = (bf16[256,2048]{1,0:T(8,128)(2,1)}, bf16[128,2048]{1,0:T(8,128)(2,1)}) custom-call(bf16[1024,2048]{1,0:T(8,128)(2,1)} %x_mix.1, bf16[2048,256]{1,0:T(8,128)(2,1)} %wq.1, bf16[2048,256]{1,0:T(8,128)(2,1)} %wk.1, bf16[2048,256]{1,0:T(8,128)(2,1)} %wv.1, bf16[2048,256]{1,0:T(8,128)(2,1)} %wo.1, bf16[512,2048]{1,0:T(8,128)(2,1)} %x_route.1, ...), custom_call_target="tpu_custom_call" | custom-call | tf_op jit(solution)/shard_map/pallas_call | solution.py:458
  129.6 2.3 %copy.22 = bf16[256,2048]{1,0:T(8,128)(2,1)} copy(bf16[256,2048]{1,0:T(8,128)(2,1)} %get-tuple-element.4) | data formatting | bytes 2097152
  131.9 1.9 %copy.23 = bf16[128,2048]{1,0:T(8,128)(2,1)} copy(bf16[128,2048]{1,0:T(8,128)(2,1)} %get-tuple-element.5) | data formatting | bytes 1048576

commit v3 on v2

--- a/solution.py
+++ b/solution.py
@@ -42,11 +42,12 @@
     mix_gain, route_gain, head_gain, w_gates, gate_bias, gate_drift, routes, weights,
     mixer_out, route_out,
     xm, wqv, wkv, wvv, wov, xr, wgv, wuv, wdv, wfull,
-    sendbuf, xin, hid, retsend, ret,
+    sendbuf, xin, hid, fsend, frecv, nsend, nrecv, psend, precv, meta_s, meta_r,
     qs, ks, vs, os_, rowsv, colsv, abuf, kvb, nb, stsend, scsend, strecv, screcv,
     cin, nin, min_, hsend, hrecv, slot_v, gate_add, gate_w,
-    lsem, own_sem, d_send, d_recv, r_send, r_recv,
+    lsem, own_sem, d_send, d_recv,
     s_send, s_recv, c_send, c_recv, h_send, h_recv, wx_send, wx_recv, wm_send, wm_recv,
+    f_send, f_recv, n_send, n_recv, p_send, p_recv, m_send, m_recv,
 ):
     e = lax.axis_index("ep")
     t = lax.axis_index("tp")
@@ -56,6 +57,12 @@
     D = xm.shape[1]
     NB = xm.shape[0] // BLK
     slots = E * cap
+    E2 = E // 2
+    span = E2 * cap
+    side = lax.div(e, E2)
+    me = lax.rem(e, E2)
+    base = side * E2
+    pal = lax.rem(e + E2, E)
     half = wd_e.shape[0] // 2
     parts = (
         (wg_e, wgv), (wu_e, wuv),
@@ -108,7 +115,9 @@
     pick = None
     for j in range(TOPK):
         slot = table[j:j + 1] * cap + jnp.sum(before * hot[j], axis=0, keepdims=True).astype(jnp.int32)
-        slot_v[j:j + 1] = slot
+        slot_v[j:j + 1] = slot - base * cap
+        meta_s[j:j + 1] = (slot - (1 - side) * span).astype(F32)
+        meta_s[TOPK + j:TOPK + j + 1] = weights[j:j + 1]
         here = (place == slot).astype(F32)
         pick = here if pick is None else pick + here
     pick = pick.astype(BF16)
@@ -125,6 +134,10 @@
 
     own = pltpu.make_async_copy(sendbuf.at[e], xin.at[e], own_sem.at[0])
     own.start()
+    meta = pltpu.make_async_remote_copy(
+        src_ref=meta_s, dst_ref=meta_r, send_sem=m_send.at[0], recv_sem=m_recv.at[0],
+        device_id=(pal, t), device_id_type=MESH)
+    meta.start()
     for k in range(1, E):
         dispatch(k).start()
     for i in range(n_parts):
@@ -265,39 +278,6 @@
             to_mate(i, k).wait_recv()
         hidden(lax.rem(mate - 2 * k + TP, TP))
 
-    for i in (2, 3):
-        for k in range(1, H):
-            across(i, k).wait_recv()
-            to_mate(i, k).start()
-    for i in (2, 3):
-        for k in range(H):
-            to_mate(i, k).wait_recv()
-
-    def give_back(k):
-        s = lax.rem(e + k, E)
-        return pltpu.make_async_remote_copy(
-            src_ref=retsend.at[s], dst_ref=ret.at[e], send_sem=r_send.at[k], recv_sem=r_recv.at[k],
-            device_id=(s, t), device_id_type=MESH)
-
-    group = max(1, 2 * LANES // cap)
-    span = group * cap
-    for n in range(E // group):
-        first = lax.rem(e // group + n + 1, E // group)
-        at = pl.ds(pl.multiple_of(first * span, span), span)
-        for c in range(0, D, CHUNK):
-            y = nn(hid[0, at, :], wdv[0, :, c:c + CHUNK])
-            for g in range(1, TP):
-                y = y + nn(hid[g, at, :], wdv[g, :, c:c + CHUNK])
-            retsend[pl.ds(first * group, group), :, c:c + CHUNK] = y.astype(BF16).reshape(group, cap, CHUNK)
-        for m in range(group):
-            s = first * group + m
-
-            @pl.when(s != e)
-            def _():
-                give_back(lax.rem(s - e + E, E)).start()
-
-    ret[e] = retsend[e]
-
     def wait_states(j, carry):
         pltpu.make_async_copy(strecv.at[j], strecv.at[j], s_recv.at[j]).wait()
         pltpu.make_async_copy(screcv.at[j], screcv.at[j], c_recv.at[j]).wait()
@@ -375,6 +355,67 @@
         share_h(k).start()
     hrecv[t] = hsend[pl.ds(pl.multiple_of(t * MR, MR), MR), :]
 
+    for i in (2, 3):
+        for k in range(1, H):
+            across(i, k).wait_recv()
+            to_mate(i, k).start()
+    for i in (2, 3):
+        for k in range(H):
+            to_mate(i, k).wait_recv()
+
+    def far(c, k):
+        m = lax.rem(me + k, E2)
+        return pltpu.make_async_remote_copy(
+            src_ref=fsend.at[c, m], dst_ref=frecv.at[c, me], send_sem=f_send.at[c, k], recv_sem=f_recv.at[c, k],
+            device_id=(base + m, t), device_id_type=MESH)
+
+    def near(k):
+        m = lax.rem(me + k, E2)
+        return pltpu.make_async_remote_copy(
+            src_ref=nsend.at[m], dst_ref=nrecv.at[me], send_sem=n_send.at[k], recv_sem=n_recv.at[k],
+            device_id=(base + m, t), device_id_type=MESH)
+
+    def part_sum(c):
+        return pltpu.make_async_remote_copy(
+            src_ref=psend.at[c], dst_ref=precv.at[c], send_sem=p_send.at[c], recv_sem=p_recv.at[c],
+            device_id=(pal, t), device_id_type=MESH)
+
+    def results(first, c):
+        at = pl.ds(pl.multiple_of(first * cap, span), span)
+        cols = slice(c * CHUNK, (c + 1) * CHUNK)
+        y = nn(hid[0, at, :], wdv[0, :, cols])
+        for g in range(1, TP):
+            y = y + nn(hid[g, at, :], wdv[g, :, cols])
+        return y.astype(BF16).reshape(E2, cap, CHUNK)
+
+    NCH = D // CHUNK
+    for c in range(NCH):
+        fsend[c] = results((1 - side) * E2, c)
+        for k in range(1, E2):
+            far(c, k).start()
+        frecv[c, me] = fsend[c, me]
+    for c in range(NCH):
+        nsend[:, :, c * CHUNK:(c + 1) * CHUNK] = results(base, c)
+    for k in range(1, E2):
+        near(k).start()
+    nrecv[me] = nsend[me]
+
+    def weigh(slot_rows, weight_rows):
+        at = lax.broadcasted_iota(jnp.int32, (span, quarter), 0).astype(slot_rows[0].dtype)
+        mat = None
+        for j in range(TOPK):
+            term = jnp.where(at == slot_rows[j], weight_rows[j], 0.0)
+            mat = term if mat is None else mat + term
+        return mat.astype(BF16)
+
+    meta.wait_recv()
+    theirs = weigh([meta_r[j:j + 1] for j in range(TOPK)], [meta_r[TOPK + j:TOPK + j + 1] for j in range(TOPK)])
+    for c in range(NCH):
+        for k in range(1, E2):
+            far(c, k).wait_recv()
+        psend[c] = tn(theirs, frecv[c].reshape(span, CHUNK)).astype(BF16)
+        part_sum(c).start()
+
     for k in range(1, H):
         across(4, k).wait_recv()
         to_mate(4, k).start()
@@ -388,20 +429,17 @@
             acc = acc + nn(hrecv[g], wfull[g, :, c:c + CHUNK])
         mixer_out[:, c:c + CHUNK] = acc.astype(BF16)
 
-    for k in range(1, E):
-        give_back(k).wait_recv()
-    mat = None
-    for j in range(TOPK):
-        term = jnp.where(place == slot_v[j:j + 1], weights[j:j + 1], 0.0)
-        mat = term if mat is None else mat + term
-    mat = mat.astype(BF16)
-    for c in range(0, D, CHUNK):
-        got = ret[:, :, c:c + CHUNK].reshape(slots, CHUNK)
-        route_out[:, c:c + CHUNK] = tn(mat, got).astype(BF16)
+    for k in range(1, E2):
+        near(k).wait_recv()
+    ours = weigh([slot_v[j:j + 1] for j in range(TOPK)], [weights[j:j + 1] for j in range(TOPK)])
+    for c in range(NCH):
+        cols = slice(c * CHUNK, (c + 1) * CHUNK)
+        kept = tn(ours, nrecv[:, :, cols].reshape(span, CHUNK))
+        part_sum(c).wait_recv()
+        route_out[:, cols] = (kept + precv[c].astype(F32)).astype(BF16)
 
     for k in range(1, E):
         dispatch(k).wait_send()
-        give_back(k).wait_send()
     for i in range(n_parts):
         for k in range(1, H):
             across(i, k).wait_send()
@@ -409,6 +447,13 @@
             to_mate(i, k).wait_send()
     for k in range(1, TP):
         share_h(k).wait_send()
+    meta.wait_send()
+    for k in range(1, E2):
+        near(k).wait_send()
+    for c in range(NCH):
+        part_sum(c).wait_send()
+        for k in range(1, E2):
+            far(c, k).wait_send()
 
     def end_states(d):
         def one(to, carry):
@@ -445,8 +490,11 @@
         V((rows, D), BF16), V((D, width), BF16), V((D, width), BF16), V((D, width), BF16), V((D, width), BF16),
         V((quarter, D), BF16), V((TP, D, FH), BF16), V((TP, D, FH), BF16), V((TP, FH, D), BF16),
         V((TP, width, D), BF16),
-        V((E, cap, D), BF16), V((E, cap, D), BF16), V((TP, E * cap, FH), BF16), V((E, cap, D), BF16),
-        V((E, cap, D), BF16),
+        V((E, cap, D), BF16), V((E, cap, D), BF16), V((TP, E * cap, FH), BF16),
+        V((D // CHUNK, E // 2, cap, CHUNK), BF16), V((D // CHUNK, E // 2, cap, CHUNK), BF16),
+        V((E // 2, cap, D), BF16), V((E // 2, cap, D), BF16),
+        V((D // CHUNK, quarter, CHUNK), BF16), V((D // CHUNK, quarter, CHUNK), BF16),
+        V((2 * TOPK, quarter), F32), V((2 * TOPK, quarter), F32),
         V((rows, width), BF16), V((rows, width), BF16), V((rows, width), BF16), V((rows, width), BF16),
         V((NB, 4 * heads, BLK), F32), V((NB, BLK, 4 * heads), F32), V((NB, 4 * heads, LANES), F32),
         V((NB, 2 * heads, HD, HD), F32), V((NB, 2 * heads, HD), F32),
@@ -454,7 +502,10 @@
         V((NB, 2 * heads, HD, HD), BF16), V((NB, 2 * heads, HD), F32), V((NB, 2 * heads, LANES), F32),
         V((rows, width), BF16), V((TP, MR, width), BF16), V((TOPK, quarter), jnp.int32), V((NB, 4 * heads, BLK), F32), V((4 * heads, D), BF16),
         dma((11,)), dma((1,)),
-    ] + [dma((E,))] * 8 + [dma((TP,))] * 2 + [dma((5, H))] * 4
+    ] + [dma((E,))] * 6 + [dma((TP,))] * 2 + [dma((5, H))] * 4 + [
+        dma((D // CHUNK, E // 2)), dma((D // CHUNK, E // 2)), dma((E // 2,)), dma((E // 2,)),
+        dma((D // CHUNK,)), dma((D // CHUNK,)), dma((1,)), dma((1,)),
+    ]
     return pl.pallas_call(
         functools.partial(body, E, TP, heads, cap, quarter),
         out_shape=(jax.ShapeDtypeStruct((MR, D), BF16), jax.ShapeDtypeStruct((quarter, D), BF16)),

time: 134 us -> 123 us (0.918)
  the two profiles are of different devices: /device:TPU:29 before, /device:TPU:0 now
where the time goes in v3:
time: 123 us; the launch traced here: 121 us
  Pallas kernels  116 us (94%)
  local copies, waits for them, and re-layouts  4.18 us (3%)
    pallas_call x1, Pallas kernels, shards(): pl.pallas_call(functools.partial(body, E, TP, heads, cap, quarter), out_s...  116 us
    unnamed x2, local copies, waits for them, and re-layouts  4.18 us

profile of v3, /device:TPU:0, one launch (start us, length us, event | category | flops | bytes accessed | tf_op | source)
XLA Modules:
  0.0 121.1 jit_solution(13684089201989223131)
XLA Ops:
  0.6 116.3 %shard_map.185 = (bf16[256,2048]{1,0:T(8,128)(2,1)}, bf16[128,2048]{1,0:T(8,128)(2,1)}) custom-call(bf16[1024,2048]{1,0:T(8,128)(2,1)} %x_mix.1, bf16[2048,256]{1,0:T(8,128)(2,1)} %wq.1, bf16[2048,256]{1,0:T(8,128)(2,1)} %wk.1, bf16[2048,256]{1,0:T(8,128)(2,1)} %wv.1, bf16[2048,256]{1,0:T(8,128)(2,1)} %wo.1, bf16[512,2048]{1,0:T(8,128)(2,1)} %x_route.1, ...), custom_call_target="tpu_custom_call" | custom-call | tf_op jit(solution)/shard_map/pallas_call | solution.py:509
  116.9 2.3 %copy.22 = bf16[256,2048]{1,0:T(8,128)(2,1)} copy(bf16[256,2048]{1,0:T(8,128)(2,1)} %get-tuple-element.4) | data formatting | bytes 2097152
  119.2 1.9 %copy.23 = bf16[128,2048]{1,0:T(8,128)(2,1)} copy(bf16[128,2048]{1,0:T(8,128)(2,1)} %get-tuple-element.5) | data formatting | bytes 1048576
